TPU v7x, 32 devices: a whole 2x2x4 slice. The times are simulated.
32 devices in a mesh: sp: 8 (over z, x), tp: 4 (over y, core).
Axes of the slice: x: 2, y: 2, z: 4, core: 2. Of those that a mesh axis runs over, the one named last changes fastest.
Arguments:
- stratum_source_matrix: bfloat16 [1024, 2048], P('sp'), may hold values from -70 to 70
- acceptance_query: bfloat16 [2, 1024, 1024], P(None, 'sp', 'tp'), may hold values from -6 to 6
- cluster_lookup_matrix: bfloat16 [2, 1024, 1024], P(None, 'sp', 'tp'), may hold values from -6 to 6
- cluster_payload_matrix: bfloat16 [2, 1024, 1024], P(None, 'sp', 'tp'), may hold values from -6 to 6
- fading_logit: bfloat16 [2, 1024, 1024], P(None, 'sp', 'tp'), may hold values from -17 to 2
- adaptation_speed_logit: bfloat16 [2, 1024, 1024], P(None, 'sp', 'tp'), may hold values from -14 to 5
- additional_fading_exponent: float32 [2, 1024, 1024], P(None, 'sp', 'tp'), may hold values from -0.7 to 0
- result_switch_pair: bfloat16 [2, 1024, 1024], P(None, 'sp', 'tp'), may hold values from -6 to 6
- attender_scaling_factor: float32 [2, 1024], P(None, 'tp'), may hold values from 0.1 to 1.9
- present_item_factor: float32 [2, 1024], P(None, 'tp'), may hold values from -0.9 to 0.9
- final_mapping_matrix: bfloat16 [2, 1024, 2048], P(None, 'tp'), may hold values from -0.125 to 0.125
- perceptron_scaling_factor: float32 [2048], replicated, may hold values from 0.1 to 1.9
- switching_matrix: bfloat16 [2048, 5632], P('sp', 'tp'), may hold values from -0.125 to 0.125
- widening_matrix: bfloat16 [2048, 5632], P('sp', 'tp'), may hold values from -0.125 to 0.125
- shrinking_matrix: bfloat16 [5632, 2048], P('tp', 'sp'), may hold values from -0.078125 to 0.078125
Outputs:
- layer_out: bfloat16 [1024, 2048], P('sp', 'tp')
All inputs are finite; a program needn't handle non-finite values.
Results may differ from a plain program's by a relative error of at most 0.014.
Values may be sent and summed in bfloat16 or wider, within the bound.
A program may use at most 128 MiB of HBM per device.

v0:
```python
import jax
import jax.numpy as jnp
from jax import lax
from jax.sharding import PartitionSpec as P

DS = 64
DL = 128
BLOCK = 64


highest = lax.Precision.HIGHEST
norm_epsilon = 1e-06
head_epsilon = 0.00064
key_epsilon = 1e-06


def entering(value, axis, combine, identity):
    devices, position = (lax.axis_size(axis), lax.axis_index(axis))
    everything = jax.tree.map(
        lambda part, kind: lax.all_gather(part.astype(kind), axis),
        value,
        jax.tree.map(lambda a: jnp.bfloat16 if a.dtype == jnp.float32 else a.dtype, value),
    )
    start = jax.tree.map(
        lambda part, zero: jnp.broadcast_to(jnp.asarray(zero, part.dtype), part.shape),
        value,
        identity,
    )

    def lap(k, before):
        reached = k < position
        new = combine(
            before, jax.tree.map(lambda part, own: part[k].astype(own.dtype), everything, value)
        )
        return jax.tree.map(lambda a, b: jnp.where(reached, a, b), new, before)

    return lax.fori_loop(0, devices, lap, start)


def per_head_terms(
    acceptance_query,
    cluster_lookup_matrix,
    cluster_payload_matrix,
    fading_logit,
    adaptation_speed_logit,
    additional_fading_exponent,
    attender_feature_count,
):
    row_count, channels = acceptance_query.shape
    lattice_layout = (row_count, channels // attender_feature_count, attender_feature_count)
    acceptance_lines = acceptance_query.astype(jnp.float32).reshape(lattice_layout)
    mapped_lookups = cluster_lookup_matrix.astype(jnp.float32).reshape(lattice_layout)
    mapped_payloads = cluster_payload_matrix.astype(jnp.float32).reshape(lattice_layout)
    learning_rate_logarithm = -jax.nn.softplus(-fading_logit.astype(jnp.float32)) - 0.5
    decay_logarithm = (additional_fading_exponent - jnp.exp(learning_rate_logarithm)).reshape(
        lattice_layout
    )
    learn_rate = jax.nn.sigmoid(adaptation_speed_logit.astype(jnp.float32)).reshape(lattice_layout)
    removal = mapped_lookups * lax.rsqrt(
        jnp.sum(mapped_lookups * mapped_lookups, axis=-1, keepdims=True) + key_epsilon
    )
    return (
        acceptance_lines,
        mapped_lookups,
        mapped_payloads,
        decay_logarithm,
        -removal,
        learn_rate * removal,
    )


def entire_cluster(
    raw_retrieval,
    acceptance_lines,
    mapped_lookups,
    mapped_payloads,
    scaling_array,
    diagonal_reward_array,
    switch_amounts,
):
    row_count, attender_count, attender_feature_count = raw_retrieval.shape
    row_mean = jnp.mean(raw_retrieval, axis=-1, keepdims=True)
    centered = raw_retrieval - row_mean
    variance = jnp.mean(centered * centered, axis=-1, keepdims=True)
    normed = (
        centered
        * lax.rsqrt(variance + head_epsilon)
        * scaling_array.reshape(attender_count, attender_feature_count)
    )
    diagonal_item_contribution = (
        jnp.sum(
            acceptance_lines
            * mapped_lookups
            * diagonal_reward_array.reshape(attender_count, attender_feature_count),
            axis=-1,
            keepdims=True,
        )
        * mapped_payloads
    )
    joined = (normed + diagonal_item_contribution).reshape(
        row_count, attender_count * attender_feature_count
    )
    return (joined * switch_amounts.astype(jnp.float32)).astype(jnp.bfloat16)


def to_blocks(array_in):
    row_count, attender_count, attender_feature_count = array_in.shape
    return array_in.reshape(
        row_count // BLOCK, BLOCK, attender_count, attender_feature_count
    ).transpose(0, 2, 1, 3)


def block_pieces(
    acceptance_lines, mapped_lookups, mapped_payloads, decay_logarithm, remove_left, remove_right
):
    (
        acceptance_lines,
        mapped_lookups,
        mapped_payloads,
        decay_logarithm,
        remove_left,
        remove_right,
    ) = [
        to_blocks(array_in)
        for array_in in (
            acceptance_lines,
            mapped_lookups,
            mapped_payloads,
            decay_logarithm,
            remove_left,
            remove_right,
        )
    ]
    attender_feature_count = acceptance_lines.shape[3]
    places = jnp.arange(BLOCK)
    inclusive = places[:, None] >= places[None, :]
    strict = places[:, None] > places[None, :]
    lower_ones = inclusive.astype(jnp.float32)
    cumulative = jnp.einsum("ts,nhsj->nhtj", lower_ones, decay_logarithm, precision=highest)
    middle = cumulative[:, :, BLOCK // 2 : BLOCK // 2 + 1, :]
    forward = jnp.exp(cumulative - middle)
    backward = jnp.exp(middle - cumulative)
    queries = jnp.concatenate(
        [remove_left * jnp.exp(-decay_logarithm) * forward, acceptance_lines * forward], axis=2
    )
    sources = jnp.concatenate([remove_right * backward, mapped_lookups * backward], axis=2)
    pair_terms = jnp.einsum("nhtj,nhsj->nhts", queries, sources, precision=highest)
    remove_remove = jnp.where(strict, pair_terms[:, :, :BLOCK, :BLOCK], 0.0)
    remove_key = jnp.where(strict, pair_terms[:, :, :BLOCK, BLOCK:], 0.0)
    read_remove = jnp.where(inclusive, pair_terms[:, :, BLOCK:, :BLOCK], 0.0)
    read_key = jnp.where(inclusive, pair_terms[:, :, BLOCK:, BLOCK:], 0.0)
    eye_block = jnp.eye(BLOCK, dtype=jnp.float32)
    targets = jnp.concatenate(
        [
            jnp.einsum("nhts,nhsj->nhtj", remove_key, mapped_payloads, precision=highest),
            remove_left * jnp.exp(cumulative - decay_logarithm),
        ],
        axis=-1,
    )
    solved = jax.scipy.linalg.solve_triangular(
        eye_block - remove_remove, targets, lower=True, unit_diagonal=True
    )
    carried_part = solved[..., :attender_feature_count]
    start_part = solved[..., attender_feature_count:]
    local_out = jnp.einsum(
        "nhts,nhsj->nhtj", read_remove, carried_part, precision=highest
    ) + jnp.einsum("nhts,nhsj->nhtj", read_key, mapped_payloads, precision=highest)
    start_read = acceptance_lines * jnp.exp(cumulative) + jnp.einsum(
        "nhts,nhsj->nhtj", read_remove, start_part, precision=highest
    )
    final_log = cumulative[:, :, BLOCK - 1 :, :]
    tail_decay = jnp.exp(final_log - cumulative)
    transit = jnp.einsum(
        "nhsi,nhsj->nhij", start_part, remove_right * tail_decay, precision=highest
    ) + jnp.eye(attender_feature_count, dtype=jnp.float32) * jnp.exp(final_log)
    added = jnp.einsum(
        "nhsi,nhsj->nhij",
        jnp.concatenate([carried_part, mapped_payloads], axis=2),
        jnp.concatenate([remove_right * tail_decay, mapped_lookups * tail_decay], axis=2),
        precision=highest,
    )
    return (local_out, start_read, transit, added)


def join_pair(earlier, later):
    return (
        jnp.einsum("hik,hkj->hij", earlier[0], later[0], precision=highest),
        jnp.einsum("hik,hkj->hij", earlier[1], later[0], precision=highest) + later[1],
    )


def join_groups(earlier, later):
    return (join_pair(earlier[0], later[0]), join_pair(earlier[1], later[1]))


def block_prefix(transit, added):
    attender_count, attender_feature_count = (transit.shape[1], transit.shape[2])
    identity_block = jnp.broadcast_to(
        jnp.eye(attender_feature_count, dtype=jnp.float32),
        (attender_count, attender_feature_count, attender_feature_count),
    )

    def advance(carried, pieces):
        return (join_pair(carried, pieces), carried)

    totals, prefixes = lax.scan(
        advance, (identity_block, jnp.zeros_like(identity_block)), (transit, added)
    )
    return (totals, prefixes)


def on_device(
    stratum_source_matrix,
    acceptance_query,
    cluster_lookup_matrix,
    cluster_payload_matrix,
    fading_logit,
    adaptation_speed_logit,
    additional_fading_exponent,
    result_switch_pair,
    attender_scaling_factor,
    present_item_factor,
    final_mapping_matrix,
    perceptron_scaling_factor,
    switching_matrix,
    widening_matrix,
    shrinking_matrix,
):
    gate_whole, up_whole = (
        lax.all_gather(switching_matrix, "sp", axis=0, tiled=True),
        lax.all_gather(widening_matrix, "sp", axis=0, tiled=True),
    )
    group_widths = (DS, DL)
    group_terms, group_pieces, group_totals, group_prefixes, identities = ([], [], [], [], [])
    for cluster_ordinal in range(2):
        aggregated_contributions = per_head_terms(
            acceptance_query[cluster_ordinal],
            cluster_lookup_matrix[cluster_ordinal],
            cluster_payload_matrix[cluster_ordinal],
            fading_logit[cluster_ordinal],
            adaptation_speed_logit[cluster_ordinal],
            additional_fading_exponent[cluster_ordinal],
            group_widths[cluster_ordinal],
        )
        local_out, start_read, transit, added = block_pieces(*aggregated_contributions)
        totals, prefixes = block_prefix(transit, added)
        group_terms.append(aggregated_contributions)
        group_pieces.append((local_out, start_read))
        group_totals.append(totals)
        group_prefixes.append(prefixes)
        identities.append(
            (
                jnp.broadcast_to(
                    jnp.eye(group_widths[cluster_ordinal], dtype=jnp.float32), totals[0].shape
                ),
                jnp.zeros_like(totals[1]),
            )
        )
    starts = entering(
        (group_totals[0], group_totals[1]), "sp", join_groups, (identities[0], identities[1])
    )
    mixed_groups = []
    for cluster_ordinal in range(2):
        acceptance_lines, mapped_lookups, mapped_payloads = (
            group_terms[cluster_ordinal][0],
            group_terms[cluster_ordinal][1],
            group_terms[cluster_ordinal][2],
        )
        row_count, attender_count, attender_feature_count = acceptance_lines.shape
        local_out, start_read = group_pieces[cluster_ordinal]
        prefix_transit, prefix_added = group_prefixes[cluster_ordinal]
        block_start = (
            jnp.einsum(
                "hik,nhkj->nhij", starts[cluster_ordinal][1], prefix_transit, precision=highest
            )
            + prefix_added
        )
        raw_retrieval = local_out + jnp.einsum(
            "nhtj,nhij->nhti", start_read, block_start, precision=highest
        )
        raw_retrieval = raw_retrieval.transpose(0, 2, 1, 3).reshape(
            row_count, attender_count, attender_feature_count
        )
        mixed_groups.append(
            entire_cluster(
                raw_retrieval,
                acceptance_lines,
                mapped_lookups,
                mapped_payloads,
                attender_scaling_factor[cluster_ordinal],
                present_item_factor[cluster_ordinal],
                result_switch_pair[cluster_ordinal],
            )
        )
    blended_result = jnp.concatenate(mixed_groups, axis=1)
    partial_value = jnp.dot(
        blended_result,
        final_mapping_matrix.reshape(-1, final_mapping_matrix.shape[2]),
        preferred_element_type=jnp.float32,
    )
    columns = perceptron_scaling_factor.shape[0] // lax.axis_size("tp")
    own_start = lax.axis_index("tp") * columns
    residual_float = stratum_source_matrix.astype(jnp.float32)
    attention = lax.psum_scatter(
        partial_value.astype(jnp.bfloat16), "tp", scatter_dimension=1, tiled=True
    ).astype(jnp.float32)
    own_residual = lax.dynamic_slice_in_dim(residual_float, own_start, columns, 1)
    own_state = (own_residual + attention).astype(jnp.bfloat16).astype(jnp.float32)
    square_total = lax.psum(jnp.sum(own_state * own_state, axis=1), "tp")
    own_gain = lax.dynamic_slice_in_dim(perceptron_scaling_factor, own_start, columns, 0)
    scaled = (
        own_state
        * lax.rsqrt(square_total / perceptron_scaling_factor.shape[0] + norm_epsilon)[:, None]
        * own_gain
    )
    normed = lax.all_gather(scaled.astype(jnp.bfloat16), "tp", axis=1, tiled=True)
    gate_pre = jnp.dot(normed, gate_whole, preferred_element_type=jnp.float32)
    up_pre = jnp.dot(normed, up_whole, preferred_element_type=jnp.float32)
    activated = (jax.nn.silu(gate_pre) * up_pre).astype(jnp.bfloat16)
    down_terms = jnp.dot(
        activated,
        lax.all_gather(shrinking_matrix, "sp", axis=1, tiled=True),
        preferred_element_type=jnp.float32,
    )
    mixer = lax.psum_scatter(
        down_terms.astype(jnp.bfloat16), "tp", scatter_dimension=1, tiled=True
    ).astype(jnp.float32)
    return (own_state + mixer).astype(jnp.bfloat16)


def solution(mesh):
    in_specs = (
        P("sp", None),
        P(None, "sp", "tp"),
        P(None, "sp", "tp"),
        P(None, "sp", "tp"),
        P(None, "sp", "tp"),
        P(None, "sp", "tp"),
        P(None, "sp", "tp"),
        P(None, "sp", "tp"),
        P(None, "tp"),
        P(None, "tp"),
        P(None, "tp", None),
        P(),
        P("sp", "tp"),
        P("sp", "tp"),
        P("tp", "sp"),
    )
    out_specs = P("sp", "tp")
    return jax.shard_map(
        on_device, mesh=mesh, in_specs=in_specs, out_specs=out_specs, check_vma=False
    )
```

profile of v0, /device:TPU:0, one launch (start us, length us, event | category | flops | bytes accessed | tf_op | source)
XLA Modules:
  0.0 649.9 jit_solution(13111955952568264399)
XLA Ops:
  15.2 1.6 fusion.183
  20.5 1.6 add_divide_fusion.1
  38.6 2.1 bitcast_multiply_fusion.12
  42.9 2.4 bitcast_multiply_fusion.3
  50.8 21.0 %custom-call.9 = f32[2,2,1,64,64]{3,4,2,1,0:T(8,128)} custom-call(f32[2,2,1,64,64]{4,3,2,1,0:T(8,128)} %fusion.117), custom_call_target="InvertDiagBlocksLowerTriangular" | custom-call | tf_op jit(solution)/shard_map/jit(_solve_triangular)/vmap(vmap())/triangular_solve | solution.py:160
  74.0 1.9 convolution_add_fusion.7
  76.8 1.6 copy.221
  79.8 2.4 fusion.91
  83.1 5.0 while.51
  88.2 35.2 %all-gather.2 = bf16[16,128,128]{2,1,0:T(8,128)(2,1)} all-gather(bf16[2,128,128]{2,1,0:T(8,128)(2,1)S(1)} %copy.239), channel_id=4, replica_groups=mesh['sp'=8,'tp'=4] {'sp'}, dimensions={0}, use_global_device_ids=true | all-gather | bytes 589824 | tf_op jit(solution)/shard_map/all_gather | solution.py:20
  123.5 33.6 %all-gather.3 = bf16[16,128,128]{2,1,0:T(8,128)(2,1)} all-gather(bf16[2,128,128]{2,1,0:T(8,128)(2,1)S(1)} %copy.240), channel_id=5, replica_groups=mesh['sp'=8,'tp'=4] {'sp'}, dimensions={0}, use_global_device_ids=true | all-gather | bytes 589824 | tf_op jit(solution)/shard_map/all_gather | solution.py:20
  157.1 40.0 %custom-call.8 = f32[2,4,1,64,64]{3,4,2,1,0:T(8,128)S(1)} custom-call(f32[2,4,1,64,64]{4,3,2,1,0:T(8,128)} %fusion.69), custom_call_target="InvertDiagBlocksLowerTriangular" | custom-call | tf_op jit(solution)/shard_map/jit(_solve_triangular)/vmap(vmap())/triangular_solve | solution.py:160
  197.2 2.2 fusion.47
  199.4 1.7 convolution_add_fusion.2
  201.1 2.4 fusion.51
  204.3 8.0 %while.50 = (s32[]{:T(128)}, f32[4,64,64]{1,2,0:T(8,128)S(1)}, f32[4,64,64]{1,2,0:T(8,128)}, f32[2,4,64,64]{2,3,1,0:T(8,128)}, f32[2,4,64,64]{2,3,1,0:T(8,128)},...) while((s32[]{:T(128)}, f32[4,64,64]{1,2,0:T(8,128)S(1)}, ...), condition=%wide.region_2.3_spmd.clone, body=%wide.region_1.2_spmd.clone.sunk | while | flops 25214980 | bytes 1443436 | solution.py:206
  205.9 1.9 fusion.227
  209.9 1.9 fusion.227
  212.3 33.4 %all-gather = bf16[32,64,64]{2,1,0:T(8,128)(2,1)} all-gather(bf16[4,64,64]{2,1,0:T(8,128)(2,1)S(1)} %copy.219), channel_id=2, replica_groups=mesh['sp'=8,'tp'=4] {'sp'}, dimensions={0}, use_global_device_ids=true | all-gather | bytes 294912 | tf_op jit(solution)/shard_map/all_gather | solution.py:20
  246.8 33.4 %all-gather.1 = bf16[32,64,64]{2,1,0:T(8,128)(2,1)} all-gather(bf16[4,64,64]{2,1,0:T(8,128)(2,1)S(1)} %copy.220), channel_id=3, replica_groups=mesh['sp'=8,'tp'=4] {'sp'}, dimensions={0}, use_global_device_ids=true | all-gather | bytes 294912 | tf_op jit(solution)/shard_map/all_gather | solution.py:20
  280.2 33.8 %while.52 = (s32[]{:T(128)}, f32[4,64,64]{1,2,0:T(8,128)S(1)}, f32[2,128,128]{1,2,0:T(8,128)S(1)}, s32[]{:T(128)}, bf16[8,4,64,64]{3,2,1,0:T(8,128)(2,1)}, /*ind...) while((s32[]{:T(128)}, f32[4,64,64]{1,2,0:T(8,128)S(1)}, ...), condition=%wide.region_7.8_spmd.clone, body=%wide.region_6.7_spmd.clone.sunk | while | flops 63160324 | bytes 1773695 | solution.py:37
  319.8 1.7 convolution_add_fusion.3
  335.0 20.4 %reduce-scatter.3.cloned.1.call-done = bf16[128,512]{1,0:T(8,128)(2,1)} async-done(((bf16[128,2048]{1,0:T(8,128)(2,1)}), bf16[128,512]{1,0:T(8,128)(2,1)}) %reduce-scatter.3.cloned.1.call-update) | async-done | bytes 131088 | tf_op jit(solution)/shard_map/reduce_scatter | solution.py:304
  356.4 6.1 psum.7
  362.6 7.2 %all_gather.44 = bf16[128,2048]{1,0:T(8,128)(2,1)S(1)} all-gather(bf16[128,512]{1,0:T(8,128)(2,1)S(1)} %fusion.58), channel_id=1, replica_groups=mesh['sp'=8,'tp'=4] {'tp'}, dimensions={1}, use_global_device_ids=true | all-gather | bytes 655360 | tf_op jit(solution)/shard_map/all_gather | solution.py:316
  369.8 58.5 %all-gather.8.cloned.1.call-done = bf16[2048,1408]{1,0:T(8,128)(2,1)} async-done(((bf16[256,1408]{1,0:T(8,128)(2,1)}), bf16[2048,1408]{1,0:T(8,128)(2,1)}) %all-gather.8.cloned.1.call-update) | async-done | bytes 5767184 | tf_op jit(solution)/shard_map/all_gather | solution.py:230
  428.3 3.6 fusion.190
  432.0 88.7 %all-gather.10.cloned.1.call-done = bf16[2048,1408]{1,0:T(8,128)(2,1)} async-done(((bf16[256,1408]{1,0:T(8,128)(2,1)}), bf16[2048,1408]{1,0:T(8,128)(2,1)}) %all-gather.10.cloned.1.call-update) | async-done | bytes 5767184 | tf_op jit(solution)/shard_map/all_gather | solution.py:231
  520.7 93.0 %all-gather.12.cloned.1.call-done = bf16[1408,2048]{1,0:T(8,128)(2,1)} async-done(((bf16[1408,256]{1,0:T(8,128)(2,1)}), bf16[1408,2048]{1,0:T(8,128)(2,1)}) %all-gather.12.cloned.1.call-update) | async-done | bytes 5767184 | tf_op jit(solution)/shard_map/all_gather | solution.py:322
  613.6 7.0 %convolution_convert_fusion.1 = bf16[128,2048]{1,0:T(8,128)(2,1)} fusion(bf16[1408,2048]{1,0:T(8,128)(2,1)} %all-gather.12.cloned.1.call-done, bf16[128,2048]{1,0:T(8,128)(2,1)S(1)} %all_gather.44, bf16[2048,1408]{1,0:T(8,128)(2,1)} %all-gather.10.cloned.1.call-done, f32[128,1408]{1,0:T(8,128)S(1)} %fusion.190), kind=kOutput, calls=%fused_computation.57 | convolution fusion | flops 1477738496 | bytes 13303808 | tf_op jit(solution)/shard_map/dot_general | solution.py:320
  620.7 20.0 %reduce-scatter.5.cloned.1.call-done = bf16[128,512]{1,0:T(8,128)(2,1)} async-done(((bf16[128,2048]{1,0:T(8,128)(2,1)}), bf16[128,512]{1,0:T(8,128)(2,1)}) %reduce-scatter.5.cloned.1.call-update) | async-done | bytes 131088 | tf_op jit(solution)/shard_map/reduce_scatter | solution.py:325
  640.7 1.6 fusion.59
  (234 shorter events, 105.4 us)
Async XLA Ops:
  7.4 323.8 %copy-start = (bf16[2,256,2048]{2,1,0:T(8,128)(2,1)S(1)}, bf16[2,256,2048]{2,1,0:T(8,128)(2,1)}, u32[]{:S(2)}) copy-start(bf16[2,256,2048]{2,1,0:T(8,128)(2,1)} %param.31) | copy-start | bytes 6291460
  7.4 348.0 %reduce-scatter.3.cloned.1.call-start = ((), (), s32[]{:S(2)}) async-start(), calls=%async_computation.2 | async-start | bytes 655360 | tf_op jit(solution)/shard_map/reduce_scatter | solution.py:304
  10.9 39.3 %copy-start.9 = (f32[64,64]{1,0:T(8,128)}, f32[64,64]{1,0:T(8,128)S(1)}, u32[]{:S(2)}) copy-start(f32[64,64]{1,0:T(8,128)S(1)} %get-tuple-element.484) | copy-start | bytes 49156
  12.6 30.4 %copy-start.4 = (f32[2,64,4,64]{1,0,3,2:T(2,128)}, f32[2,64,4,64]{1,0,3,2:T(2,128)S(1)}, u32[]{:S(2)}) copy-start(f32[2,64,4,64]{1,0,3,2:T(2,128)S(1)} %reshape.261) | copy-start | bytes 393220
  18.8 0.7 copy-start.11
  19.6 25.8 %copy-start.6 = (f32[2,64,2,128]{3,2,1,0:T(2,128)}, f32[2,64,2,128]{3,2,1,0:T(2,128)S(1)}, u32[]{:S(2)}) copy-start(f32[2,64,2,128]{3,2,1,0:T(2,128)S(1)} %reshape.251) | copy-start | bytes 393220
  25.9 20.7 %copy-start.7 = (bf16[2,64,2,128]{3,2,1,0:T(2,128)(2,1)}, bf16[2,64,2,128]{3,2,1,0:T(2,128)(2,1)S(1)}, u32[]{:S(2)}) copy-start(bf16[2,64,2,128]{3,2,1,0:T(2,128)(2,1)S(1)} %reshape_reshape.5) | copy-start | bytes 196612
  26.8 9.9 %copy-start.8 = (f32[2,64,4,64]{1,3,2,0:T(8,128)}, f32[2,64,4,64]{1,3,2,0:T(8,128)S(1)}, u32[]{:S(2)}) copy-start(f32[2,64,4,64]{1,3,2,0:T(8,128)S(1)} %copy.193) | copy-start | bytes 393220
  30.2 15.1 %copy-start.1 = (f32[2,4,64,64]{2,3,1,0:T(8,128)}, f32[2,4,64,64]{2,3,1,0:T(8,128)S(1)}, u32[]{:S(2)}) copy-start(f32[2,4,64,64]{2,3,1,0:T(8,128)S(1)} %convolution_bitcast_fusion.8) | copy-start | bytes 393220
  41.3 37.0 %copy-start.3 = (f32[2,2,128,128]{3,2,1,0:T(8,128)}, f32[2,2,128,128]{3,2,1,0:T(8,128)S(1)}, u32[]{:S(2)}) copy-start(f32[2,2,128,128]{3,2,1,0:T(8,128)S(1)} %fusion.80) | copy-start | bytes 786436
  48.2 2.6 copy-start.5
  83.1 116.3 %copy-start.10 = (f32[64,64]{1,0:T(8,128)S(1)}, f32[64,64]{1,0:T(8,128)}, u32[]{:S(2)}) copy-start(f32[64,64]{1,0:T(8,128)} %copy-done.9) | copy-start | bytes 49156
  83.1 116.3 %copy-start.16 = (f32[2,4,64]{2,1,0:T(4,128)S(1)}, f32[2,4,64]{2,1,0:T(4,128)}, u32[]{:S(2)}) copy-start(f32[2,4,64]{2,1,0:T(4,128)} %get-tuple-element.382) | copy-start | bytes 6148
  280.2 39.6 %copy-start.2 = (f32[2,4,64,64]{2,3,1,0:T(8,128)S(1)}, f32[2,4,64,64]{2,3,1,0:T(8,128)}, u32[]{:S(2)}) copy-start(f32[2,4,64,64]{2,3,1,0:T(8,128)} %copy-done.1) | copy-start | bytes 393220
  314.0 13.8 %copy-start.12 = (f32[1,128,256]{2,1,0:T(8,128)S(1)}, f32[1,128,256]{2,1,0:T(8,128)}, u32[]{:S(2)}) copy-start(f32[1,128,256]{2,1,0:T(8,128)} %get-tuple-element.471) | copy-start | bytes 393220
  319.8 7.6 %copy-start.13 = (f32[1,128,256]{1,2,0:T(8,128)S(1)}, f32[1,128,256]{1,2,0:T(8,128)}, u32[]{:S(2)}) copy-start(f32[1,128,256]{1,2,0:T(8,128)} %get-tuple-element.472) | copy-start | bytes 393220
  321.5 8.7 %copy-start.14 = (bf16[2,128,256]{2,1,0:T(8,128)(2,1)S(1)}, bf16[2,128,256]{2,1,0:T(8,128)(2,1)}, u32[]{:S(2)}) copy-start(bf16[2,128,256]{2,1,0:T(8,128)(2,1)} %param.24) | copy-start | bytes 393220
  321.5 8.7 %copy-start.15 = (f32[2,64,2,128]{3,2,1,0:T(2,128)S(1)}, f32[2,64,2,128]{3,2,1,0:T(2,128)}, u32[]{:S(2)}) copy-start(f32[2,64,2,128]{3,2,1,0:T(2,128)} %copy.256) | copy-start | bytes 393220
  332.4 95.9 %all-gather.8.cloned.1.call-start = ((), (), s32[]{:S(2)}) async-start(), calls=%async_computation.3 | async-start | bytes 6488064 | tf_op jit(solution)/shard_map/all_gather | solution.py:230
  333.0 187.7 %all-gather.10.cloned.1.call-start = ((), (), s32[]{:S(2)}) async-start(), calls=%async_computation.4 | async-start | bytes 6488064 | tf_op jit(solution)/shard_map/all_gather | solution.py:231
  333.6 280.1 %all-gather.12.cloned.1.call-start = ((), (), s32[]{:S(2)}) async-start(), calls=%async_computation.5 | async-start | bytes 6488064 | tf_op jit(solution)/shard_map/all_gather | solution.py:322
  334.1 306.6 %reduce-scatter.5.cloned.1.call-start = ((), (), s32[]{:S(2)}) async-start(), calls=%async_computation.6 | async-start | bytes 655360 | tf_op jit(solution)/shard_map/reduce_scatter | solution.py:325
Sparse Core Ops, SparseCore 0:
  332.5 22.7 reduce-scatter.2
  620.8 19.8 reduce-scatter.4
Sparse Core Ops, SparseCore 1:
  335.1 93.2 all-gather.7
  430.4 90.2 all-gather.9
  522.6 91.0 all-gather.11
where the time goes:
time: 653 us; the launch traced here: 650 us
  waiting for transfers between devices  282 us (43%)
  blocking collectives  149 us (23%)
  other arithmetic  87.6 us (13%)
  matrix products  68.4 us (10%)
  local copies, waits for them, and re-layouts  46.4 us (7%)
  between operations  15.6 us (2%)
    all_gather x4, blocking collectives, entering(): lax.all_gather(part.astype(kind), axis)  136 us
    all_gather x1, waiting for transfers between devices, on_device(): lax.all_gather(shrinking_matrix, 'sp', axis=1, tiled=True)  93 us
    all_gather x1, waiting for transfers between devices, on_device(): lax.all_gather(widening_matrix, 'sp', axis=0, tiled=True)  88.7 us
    another operation x5, other arithmetic, block_pieces(): jax.scipy.linalg.solve_triangular(eye_block - remove_remove, targets, low...  63.1 us
    all_gather x1, waiting for transfers between devices, on_device(): lax.all_gather(switching_matrix, 'sp', axis=0, tiled=True)  58.5 us
    dot_general x20, matrix products, join_pair(): jnp.einsum('hik,hkj->hij', earlier[1], later[0], precision=highest)  24.2 us
    reduce_scatter x1, waiting for transfers between devices, on_device(): lax.psum_scatter(partial_value.astype(jnp.bfloat16), 'tp', scatter_dimens...  20.4 us
    reduce_scatter x1, waiting for transfers between devices, on_device(): lax.psum_scatter(down_terms.astype(jnp.bfloat16), 'tp', scatter_dimension...  20 us
  transfers between devices with their start and end apart: 5, of which 5 were waited for; matrix products, arithmetic and copies ran while one was open for 1% of the time, Pallas kernels for 0%

commit v1 on v0

v1 whole, which is shorter than its diff:
```python
import functools

import jax
import jax.numpy as jnp
from jax import lax
from jax.experimental import pallas as pl
from jax.experimental.pallas import tpu as pltpu
from jax.sharding import PartitionSpec as P

DS = 64
DL = 128
LANES = 128
MESH = pl.DeviceIdType.MESH

norm_epsilon = 1e-06
head_epsilon = 0.00064
key_epsilon = 1e-06


NN = (((1,), (0,)), ((), ()))
NT = (((1,), (1,)), ((), ()))


def split(x, count=2):
    if x.dtype == jnp.bfloat16:
        return [x]
    parts = []
    for _ in range(count - 1):
        high = x.astype(jnp.bfloat16)
        parts.append(high)
        x = x - high.astype(jnp.float32)
    return parts + [x.astype(jnp.bfloat16)]


def product(a, b, dims, count=2):
    total = None
    for i, p in enumerate(split(a, count)):
        for j, r in enumerate(split(b, count)):
            if i + j < count:
                term = lax.dot_general(p, r, dims, preferred_element_type=jnp.float32)
                total = term if total is None else total + term
    return total


def mm(a, b, count=2):
    return product(a, b, NN, count)


def mm_nt(a, b):
    return product(a, b, NT)


def sigmoid(x):
    return 1.0 / (1.0 + jnp.exp(-x))


def same_head(width):
    i = lax.broadcasted_iota(jnp.int32, (LANES, LANES), 0) // width
    j = lax.broadcasted_iota(jnp.int32, (LANES, LANES), 1) // width
    return (i == j).astype(jnp.float32).astype(jnp.bfloat16)


def unit_inverse(strict_part, rows, cols):
    size = strict_part.shape[0]
    inverse = (rows == cols).astype(jnp.float32)
    half = 1
    while half < size:
        off = (rows // (2 * half) == cols // (2 * half)) & (rows // half != cols // half)
        part = jnp.where(off, strict_part, 0.0)
        if half == 1:
            inverse = inverse + part
        else:
            inverse = inverse + mm(mm(inverse, part), inverse)
        half *= 2
    return inverse


def local_unit(width, q, k, v, fade, speed, extra):
    T = q.shape[0]
    ones = same_head(width)
    log_decay = extra - jnp.exp(jnp.float32(-0.5)) * sigmoid(fade)
    removal = k * lax.rsqrt(mm(k * k, ones) + key_epsilon)
    left = -removal
    right = sigmoid(speed) * removal
    rows = lax.broadcasted_iota(jnp.int32, (T, T), 0)
    cols = lax.broadcasted_iota(jnp.int32, (T, T), 1)
    inclusive = rows >= cols
    strict = rows > cols
    cumulative = mm(inclusive.astype(jnp.float32).astype(jnp.bfloat16), log_decay, 3)
    middle = cumulative[T // 2 : T // 2 + 1, :]
    final = cumulative[T - 1 : T, :]
    forward = jnp.exp(cumulative - middle)
    backward = jnp.exp(middle - cumulative)
    tail = jnp.exp(final - cumulative)
    queries = jnp.concatenate([left * jnp.exp(-log_decay) * forward, q * forward], axis=0)
    sources = jnp.concatenate([right * backward, k * backward], axis=0)
    start_target = left * jnp.exp(cumulative - log_decay)
    right_tail = right * tail
    key_tail = k * tail
    eye = lax.broadcasted_iota(jnp.int32, (LANES, LANES), 0) == lax.broadcasted_iota(
        jnp.int32, (LANES, LANES), 1
    )
    transit = jnp.where(eye, jnp.exp(final), 0.0)
    start_read = q * jnp.exp(cumulative)
    added = jnp.zeros((LANES, LANES), jnp.float32)
    local_out = jnp.zeros((T, LANES), jnp.float32)
    lane = lax.broadcasted_iota(jnp.int32, (1, LANES), 1) // width
    for head in range(LANES // width):
        only = lane == head
        pick = (lambda a: a) if width == LANES else (lambda a: jnp.where(only, a, 0.0))
        pairs = mm_nt(pick(queries), sources)
        remove_remove = jnp.where(strict, pairs[:T, :T], 0.0)
        remove_key = jnp.where(strict, pairs[:T, T:], 0.0)
        read_remove = jnp.where(inclusive, pairs[T:, :T], 0.0)
        read_key = jnp.where(inclusive, pairs[T:, T:], 0.0)
        inverse = unit_inverse(remove_remove, rows, cols)
        value = pick(v)
        carried = mm(inverse, mm(remove_key, value))
        start = mm(inverse, pick(start_target))
        local_out = local_out + mm(read_remove, carried) + mm(read_key, value)
        start_read = start_read + mm(read_remove, start)
        head_right = pick(right_tail)
        transit = transit + mm(start.T, head_right)
        added = added + mm(carried.T, head_right) + mm(value.T, pick(key_tail))
    return local_out, start_read, transit, added


def finish_unit(width, read, q, k, v, gain, own, gate):
    ones = same_head(width)
    mean = mm(read, ones) / width
    centered = read - mean
    variance = mm(centered * centered, ones) / width
    normed = centered * lax.rsqrt(variance + head_epsilon) * gain
    diagonal = mm(q * k * own, ones) * v
    return ((normed + diagonal) * gate).astype(jnp.bfloat16)


def attention_kernel(
    n_sp, widths, q_ref, k_ref, v_ref, f_ref, a_ref, e_ref, g_ref, gain_ref, own_ref,
    mixed_ref, local_ref, read_ref, mine, got, send_sem, recv_sem,
):
    me = lax.axis_index("sp")
    tp = lax.axis_index("tp")

    barrier = pltpu.get_barrier_semaphore()

    @pl.loop(1, n_sp)
    def _(d):
        pl.semaphore_signal(
            barrier, inc=1, device_id=(lax.rem(me + d, n_sp), tp), device_id_type=MESH
        )

    pl.semaphore_wait(barrier, n_sp - 1)

    per_group = q_ref.shape[2] // LANES

    def load(ref, g, c):
        return ref[g, :, c * LANES : (c + 1) * LANES].astype(jnp.float32)

    def copy(u, d, to):
        return pltpu.make_async_remote_copy(
            src_ref=mine.at[u],
            dst_ref=got.at[d, u],
            send_sem=send_sem.at[u, d],
            recv_sem=recv_sem.at[u, d],
            device_id=(to, tp),
            device_id_type=MESH,
        )

    units = [(g, c) for g in range(2) for c in range(per_group)]
    for u, (g, c) in enumerate(units):
        local_out, start_read, transit, added = local_unit(
            widths[g], *(load(r, g, c) for r in (q_ref, k_ref, v_ref, f_ref, a_ref, e_ref))
        )
        local_ref[u] = local_out
        read_ref[u] = start_read
        mine[u, 0] = transit.astype(jnp.bfloat16)
        mine[u, 1] = added.astype(jnp.bfloat16)

        @pl.loop(1, n_sp)
        def _(d):
            @pl.when(me + d < n_sp)
            def _():
                copy(u, d, me + d).start()

    for u in range(len(units)):

        @pl.loop(1, n_sp)
        def _(d):
            @pl.when(me - d >= 0)
            def _():
                copy(u, d, me).wait_recv()

    def fold(step, states):
        d = me - step
        return tuple(
            mm(s, got[d, u, 0]) + got[d, u, 1].astype(jnp.float32)
            for u, s in enumerate(states)
        )

    states = lax.fori_loop(
        0, me, fold, tuple(jnp.zeros((LANES, LANES), jnp.float32) for _ in units)
    )
    for u, (g, c) in enumerate(units):
        lanes = slice(c * LANES, (c + 1) * LANES)
        read = local_ref[u] + mm_nt(read_ref[u], states[u])
        mixed = finish_unit(
            widths[g], read, load(q_ref, g, c), load(k_ref, g, c), load(v_ref, g, c),
            gain_ref[g : g + 1, lanes], own_ref[g : g + 1, lanes], load(g_ref, g, c),
        )
        mixed_ref[:, u * LANES : (u + 1) * LANES] = mixed

    for u in range(len(units)):

        @pl.loop(1, n_sp)
        def _(d):
            @pl.when(me + d < n_sp)
            def _():
                copy(u, d, me + d).wait_send()


def attention(n_sp, q, k, v, f, a, e, g, gain, own):
    T, channels = q.shape[1], q.shape[2]
    units = 2 * channels // LANES
    vmem = pl.BlockSpec(memory_space=pltpu.VMEM)
    return pl.pallas_call(
        functools.partial(attention_kernel, n_sp, (DS, DL)),
        out_shape=jax.ShapeDtypeStruct((T, 2 * channels), jnp.bfloat16),
        in_specs=[vmem] * 9,
        out_specs=vmem,
        scratch_shapes=[
            pltpu.VMEM((units, T, LANES), jnp.float32),
            pltpu.VMEM((units, T, LANES), jnp.float32),
            pltpu.VMEM((units, 2, LANES, LANES), jnp.bfloat16),
            pltpu.VMEM((n_sp, units, 2, LANES, LANES), jnp.bfloat16),
            pltpu.SemaphoreType.DMA((units, n_sp)),
            pltpu.SemaphoreType.DMA((units, n_sp)),
        ],
        compiler_params=pltpu.CompilerParams(
            collective_id=0, has_side_effects=True, vmem_limit_bytes=40 * 2**20
        ),
        cost_estimate=pl.CostEstimate(
            flops=4 * 10**8, bytes_accessed=2**21, transcendentals=0
        ),
        name="attention",
    )(q, k, v, f, a, e, g, gain, own)


def on_device(
    stratum_source_matrix,
    acceptance_query,
    cluster_lookup_matrix,
    cluster_payload_matrix,
    fading_logit,
    adaptation_speed_logit,
    additional_fading_exponent,
    result_switch_pair,
    attender_scaling_factor,
    present_item_factor,
    final_mapping_matrix,
    perceptron_scaling_factor,
    switching_matrix,
    widening_matrix,
    shrinking_matrix,
):
    gate_whole, up_whole = (
        lax.all_gather(switching_matrix, "sp", axis=0, tiled=True),
        lax.all_gather(widening_matrix, "sp", axis=0, tiled=True),
    )
    mixed = attention(
        lax.axis_size("sp"),
        acceptance_query,
        cluster_lookup_matrix,
        cluster_payload_matrix,
        fading_logit,
        adaptation_speed_logit,
        additional_fading_exponent,
        result_switch_pair,
        attender_scaling_factor,
        present_item_factor,
    )
    partial_value = jnp.dot(
        mixed,
        final_mapping_matrix.reshape(-1, final_mapping_matrix.shape[2]),
        preferred_element_type=jnp.float32,
    )
    columns = perceptron_scaling_factor.shape[0] // lax.axis_size("tp")
    own_start = lax.axis_index("tp") * columns
    residual_float = stratum_source_matrix.astype(jnp.float32)
    branch = lax.psum_scatter(
        partial_value.astype(jnp.bfloat16), "tp", scatter_dimension=1, tiled=True
    ).astype(jnp.float32)
    own_residual = lax.dynamic_slice_in_dim(residual_float, own_start, columns, 1)
    own_state = (own_residual + branch).astype(jnp.bfloat16).astype(jnp.float32)
    square_total = lax.psum(jnp.sum(own_state * own_state, axis=1), "tp")
    own_gain = lax.dynamic_slice_in_dim(perceptron_scaling_factor, own_start, columns, 0)
    scaled = (
        own_state
        * lax.rsqrt(square_total / perceptron_scaling_factor.shape[0] + norm_epsilon)[:, None]
        * own_gain
    )
    normed = lax.all_gather(scaled.astype(jnp.bfloat16), "tp", axis=1, tiled=True)
    gate_pre = jnp.dot(normed, gate_whole, preferred_element_type=jnp.float32)
    up_pre = jnp.dot(normed, up_whole, preferred_element_type=jnp.float32)
    activated = (jax.nn.silu(gate_pre) * up_pre).astype(jnp.bfloat16)
    down_terms = jnp.dot(
        activated,
        lax.all_gather(shrinking_matrix, "sp", axis=1, tiled=True),
        preferred_element_type=jnp.float32,
    )
    mixer = lax.psum_scatter(
        down_terms.astype(jnp.bfloat16), "tp", scatter_dimension=1, tiled=True
    ).astype(jnp.float32)
    return (own_state + mixer).astype(jnp.bfloat16)


def solution(mesh):
    tokens = P(None, "sp", "tp")
    in_specs = (
        P("sp", None), tokens, tokens, tokens, tokens, tokens, tokens, tokens,
        P(None, "tp"), P(None, "tp"), P(None, "tp", None), P(),
        P("sp", "tp"), P("sp", "tp"), P("tp", "sp"),
    )
    return jax.shard_map(
        on_device, mesh=mesh, in_specs=in_specs, out_specs=P("sp", "tp"), check_vma=False
    )
```

time: 653 us -> 394 us (0.60)
  blocking collectives: 149 us -> 13.2 us
  other arithmetic: 87.6 us -> 2.8 us
  matrix products: 68.4 us -> 11.9 us
  Pallas kernels: 0 us -> 45.9 us
  local copies, waits for them, and re-layouts: 46.4 us -> 8.65 us
  waiting for transfers between devices: 282 us -> 296 us
    all_gather x4 -> x0, blocking collectives: 136 us -> none  [entering(): lax.all_gather(part.astype(kind), axis)]
    another operation x7 -> x0, other arithmetic: 63.1 us -> none  [the longest x5 63.1 us: block_pieces(): jax.scipy.linalg.solve_triangular(eye_block - remove_remove, targets, low...]
    dot_general x45 -> x1, matrix products: 54.1 us -> 1.26 us  [on_device(): jnp.dot(mixed, final_mapping_matrix.reshape(-1, final_mapping_matrix.shap...]
    pallas_call x0 -> x1, Pallas kernels: none -> 45.9 us  [attention(): pl.pallas_call(functools.partial(attention_kernel, n_sp, (DS, DL)), out_s...]
    dynamic_slice x32 -> x0, local copies, waits for them, and re-layouts: 15.4 us -> none  [lap(): part[k].astype(own.dtype)]
    reduce_scatter x1, waiting for transfers between devices: 20.4 us -> 34.4 us  [on_device(): lax.psum_scatter(partial_value.astype(jnp.bfloat16), 'tp', scatter_dimens...]
    unnamed x36 -> x20, local copies, waits for them, and re-layouts: 0.3 us -> 7.89 us
    mul x6 -> x0, other arithmetic: 7.4 us -> none  [the longest x1 2.4 us: block_pieces(): remove_right * backward]
where the time goes in v1:
time: 394 us
  waiting for transfers between devices  296 us (75%)
  Pallas kernels  45.9 us (12%)
  between operations  15.1 us (4%)
  blocking collectives  13.2 us (3%)
  matrix products  11.9 us (3%)
  local copies, waits for them, and re-layouts  8.65 us (2%)
    all_gather x1, waiting for transfers between devices, on_device(): lax.all_gather(shrinking_matrix, 'sp', axis=1, tiled=True)  93 us
    all_gather x1, waiting for transfers between devices, on_device(): lax.all_gather(widening_matrix, 'sp', axis=0, tiled=True)  88.7 us
    all_gather x1, waiting for transfers between devices, on_device(): lax.all_gather(switching_matrix, 'sp', axis=0, tiled=True)  58.6 us
    pallas_call x1, Pallas kernels, attention(): pl.pallas_call(functools.partial(attention_kernel, n_sp, (DS, DL)), out_s...  45.9 us
    reduce_scatter x1, waiting for transfers between devices, on_device(): lax.psum_scatter(partial_value.astype(jnp.bfloat16), 'tp', scatter_dimens...  34.4 us
    reduce_scatter x1, waiting for transfers between devices, on_device(): lax.psum_scatter(down_terms.astype(jnp.bfloat16), 'tp', scatter_dimension...  20 us
    unnamed x20, local copies, waits for them, and re-layouts  7.89 us
  transfers between devices with their start and end apart: 5, of which 5 were waited for; matrix products, arithmetic and copies ran while one was open for 1% of the time, Pallas kernels for 0%

profile of v1, /device:TPU:0, one launch (start us, length us, event | category | flops | bytes accessed | tf_op | source)
XLA Modules:
  0.0 394.0 jit_solution(17036354908236698652)
XLA Ops:
  7.4 1.1 copy-done.1
  8.5 0.9 copy-done.2
  9.4 0.9 copy-done.3
  10.3 0.9 copy-done.4
  11.2 0.9 copy-done.5
  12.1 0.9 copy-done.6
  13.0 0.9 copy-done.7
  13.9 0.7 copy-done.8
  14.6 0.7 copy-done.9
  15.3 45.9 %attention.1 = bf16[128,512]{1,0:T(8,128)(2,1)S(1)} custom-call(bf16[2,128,256]{2,1,0:T(8,128)(2,1)S(1)} %copy-done.2, bf16[2,128,256]{2,1,0:T(8,128)(2,1)S(1)} %copy-done.3, bf16[2,128,256]{2,1,0:T(8,128)(2,1)S(1)} %copy-done.4, bf16[2,128,256]{2,1,0:T(8,128)(2,1)S(1)} %copy-done.5, bf16[2,128,256]{2,1,0:T(8,128)(2,1)S(1)} %copy-done.6, ...), custom_call_target="tpu_custom_call" | custom-call | flops 400000000 | bytes 2097152 | tf_op jit(solution)/shard_map/attention/pallas_call | solution.py:226
  61.2 1.3 convolution_convert_fusion
  62.4 0.0 reduce-scatter.3.cloned.1.call-update
  62.5 0.0 all-gather.4.cloned.1.call-start
  62.5 0.5 all-gather.4.cloned.1.call-update
  63.0 0.0 all-gather.6.cloned.1.call-start
  63.1 0.5 all-gather.6.cloned.1.call-update
  63.6 0.0 all-gather.8.cloned.1.call-start
  63.7 0.5 all-gather.8.cloned.1.call-update
  64.2 0.0 reduce-scatter.5.cloned.1.call-start
  64.3 0.8 dynamic_slice.7
  65.0 34.4 %reduce-scatter.3.cloned.1.call-done = bf16[128,512]{1,0:T(8,128)(2,1)} async-done(((bf16[128,2048]{1,0:T(8,128)(2,1)}), bf16[128,512]{1,0:T(8,128)(2,1)}) %reduce-scatter.3.cloned.1.call-update) | async-done | bytes 131088 | tf_op jit(solution)/shard_map/reduce_scatter | solution.py:290
  99.4 1.1 fusion.2
  100.5 6.1 %psum.7 = f32[128]{0:T(128)S(1)} all-reduce(f32[128]{0:T(128)S(1)} %get-tuple-element.5), channel_id=1, replica_groups=mesh['sp'=8,'tp'=4] {'tp'}, use_global_device_ids=true, to_apply=%region_2.0 | all-reduce | flops 128 | bytes 1024 | tf_op jit(solution)/shard_map/psum | solution.py:295
  106.6 0.1 fusion.4
  106.7 7.2 %all_gather.12 = bf16[128,2048]{1,0:T(8,128)(2,1)S(1)} all-gather(bf16[128,512]{1,0:T(8,128)(2,1)S(1)} %fusion.4), channel_id=1, replica_groups=mesh['sp'=8,'tp'=4] {'tp'}, dimensions={1}, use_global_device_ids=true | all-gather | bytes 655360 | tf_op jit(solution)/shard_map/all_gather | solution.py:302
  113.8 58.6 %all-gather.4.cloned.1.call-done = bf16[2048,1408]{1,0:T(8,128)(2,1)} async-done(((bf16[256,1408]{1,0:T(8,128)(2,1)}), bf16[2048,1408]{1,0:T(8,128)(2,1)}) %all-gather.4.cloned.1.call-update) | async-done | bytes 5767184 | tf_op jit(solution)/shard_map/all_gather | solution.py:267
  172.4 3.6 fusion.7
  176.0 88.7 %all-gather.6.cloned.1.call-done = bf16[2048,1408]{1,0:T(8,128)(2,1)} async-done(((bf16[256,1408]{1,0:T(8,128)(2,1)}), bf16[2048,1408]{1,0:T(8,128)(2,1)}) %all-gather.6.cloned.1.call-update) | async-done | bytes 5767184 | tf_op jit(solution)/shard_map/all_gather | solution.py:268
  264.7 93.0 %all-gather.8.cloned.1.call-done = bf16[1408,2048]{1,0:T(8,128)(2,1)} async-done(((bf16[1408,256]{1,0:T(8,128)(2,1)}), bf16[1408,2048]{1,0:T(8,128)(2,1)}) %all-gather.8.cloned.1.call-update) | async-done | bytes 5767184 | tf_op jit(solution)/shard_map/all_gather | solution.py:308
  357.7 7.1 %convolution_convert_fusion.1 = bf16[128,2048]{1,0:T(8,128)(2,1)} fusion(bf16[1408,2048]{1,0:T(8,128)(2,1)} %all-gather.8.cloned.1.call-done, bf16[128,2048]{1,0:T(8,128)(2,1)S(1)} %all_gather.12, bf16[2048,1408]{1,0:T(8,128)(2,1)} %all-gather.6.cloned.1.call-done, f32[128,1408]{1,0:T(8,128)S(1)} %fusion.7), kind=kOutput, calls=%fused_computation.3 | convolution fusion | flops 1477738496 | bytes 13303808 | tf_op jit(solution)/shard_map/dot_general | solution.py:306
  364.8 20.0 %reduce-scatter.5.cloned.1.call-done = bf16[128,512]{1,0:T(8,128)(2,1)} async-done(((bf16[128,2048]{1,0:T(8,128)(2,1)}), bf16[128,512]{1,0:T(8,128)(2,1)}) %reduce-scatter.5.cloned.1.call-update) | async-done | bytes 131088 | tf_op jit(solution)/shard_map/reduce_scatter | solution.py:311
  384.8 1.6 fusion.5
  (14 shorter events, 0.0 us)
Async XLA Ops:
  7.4 53.8 %copy-start = (bf16[2,256,2048]{2,1,0:T(8,128)(2,1)S(1)}, bf16[2,256,2048]{2,1,0:T(8,128)(2,1)}, u32[]{:S(2)}) copy-start(bf16[2,256,2048]{2,1,0:T(8,128)(2,1)} %param.25) | copy-start | bytes 6291460
  7.4 92.0 %reduce-scatter.3.cloned.1.call-start = ((), (), s32[]{:S(2)}) async-start(), calls=%async_computation.2 | async-start | bytes 655360 | tf_op jit(solution)/shard_map/reduce_scatter | solution.py:290
  7.4 1.1 copy-start.1
  8.5 0.9 copy-start.2
  9.4 0.9 copy-start.3
  10.3 0.9 copy-start.4
  11.2 0.9 copy-start.5
  12.1 0.9 copy-start.6
  13.0 0.9 copy-start.7
  13.9 0.7 copy-start.8
  14.6 0.7 copy-start.9
  62.5 109.9 %all-gather.4.cloned.1.call-start = ((), (), s32[]{:S(2)}) async-start(), calls=%async_computation.3 | async-start | bytes 6488064 | tf_op jit(solution)/shard_map/all_gather | solution.py:267
  63.0 201.7 %all-gather.6.cloned.1.call-start = ((), (), s32[]{:S(2)}) async-start(), calls=%async_computation.4 | async-start | bytes 6488064 | tf_op jit(solution)/shard_map/all_gather | solution.py:268
  63.6 294.1 %all-gather.8.cloned.1.call-start = ((), (), s32[]{:S(2)}) async-start(), calls=%async_computation.5 | async-start | bytes 6488064 | tf_op jit(solution)/shard_map/all_gather | solution.py:308
  64.2 320.6 %reduce-scatter.5.cloned.1.call-start = ((), (), s32[]{:S(2)}) async-start(), calls=%async_computation.6 | async-start | bytes 655360 | tf_op jit(solution)/shard_map/reduce_scatter | solution.py:311
Sparse Core Ops, SparseCore 0:
  62.6 36.7 reduce-scatter.2
  364.9 19.8 reduce-scatter.4
Sparse Core Ops, SparseCore 1:
  65.1 107.2 all-gather.3
  174.4 90.3 all-gather.5
  266.7 91.0 all-gather.7

commit v2 on v1

--- a/solution.py
+++ b/solution.py
@@ -137,7 +137,9 @@
 
 def attention_kernel(
     n_sp, widths, q_ref, k_ref, v_ref, f_ref, a_ref, e_ref, g_ref, gain_ref, own_ref,
-    mixed_ref, local_ref, read_ref, mine, got, send_sem, recv_sem,
+    first_ref, second_ref, mixed_ref, first_out, second_out,
+    local_ref, read_ref, mine, got, send_sem, recv_sem,
+    up_sem, down_sem, along_sem, side_sem, side_recv, keep_sem,
 ):
     me = lax.axis_index("sp")
     tp = lax.axis_index("tp")
@@ -151,6 +153,64 @@
         )
 
     pl.semaphore_wait(barrier, n_sp - 1)
+
+    line, side = me // 2, me % 2
+    length = n_sp // 2
+    weights = ((first_ref, first_out), (second_ref, second_out))
+
+    def pass_on(w, block, to, source, sem, landed):
+        return pltpu.make_async_remote_copy(
+            src_ref=source, dst_ref=weights[w][1].at[block], send_sem=sem, recv_sem=landed,
+            device_id=(to, tp), device_id_type=MESH,
+        )
+
+    def to_line(w, at, to, source, sem):
+        return pass_on(w, at * 2 + side, to * 2 + side, source, sem.at[w, at], along_sem.at[w, at])
+
+    def to_side(w, at, source):
+        return pass_on(
+            w, at * 2 + side, line * 2 + 1 - side, source, side_sem.at[w, at], side_recv.at[w, at]
+        )
+
+    def spread(w, at, source, upward, downward):
+        if upward:
+
+            @pl.when(line + 1 < length)
+            def _():
+                to_line(w, at, line + 1, source, up_sem).start()
+
+        if downward:
+
+            @pl.when(line >= 1)
+            def _():
+                to_line(w, at, line - 1, source, down_sem).start()
+
+        to_side(w, at, source).start()
+
+    def relay(i):
+        for w in range(2):
+            below, above = line - i, line + i
+
+            @pl.when(below >= 0)
+            def _():
+                source = weights[w][1].at[below * 2 + side]
+                to_line(w, below, line, source, up_sem).wait_recv()
+                spread(w, below, source, True, False)
+
+            @pl.when(above < length)
+            def _():
+                source = weights[w][1].at[above * 2 + side]
+                to_line(w, above, line, source, down_sem).wait_recv()
+                spread(w, above, source, False, True)
+
+    for w in range(2):
+        spread(w, line, weights[w][0], True, True)
+    keeps = [
+        pltpu.make_async_copy(weights[w][0], weights[w][1].at[me], keep_sem.at[w])
+        for w in range(2)
+    ]
+    for keep in keeps:
+        keep.start()
 
     per_group = q_ref.shape[2] // LANES
 
@@ -183,6 +243,11 @@
             def _():
                 copy(u, d, me + d).start()
 
+        if u == 1 and length > 1:
+            relay(1)
+        if u == 3 and length > 2:
+            relay(2)
+
     for u in range(len(units)):
 
         @pl.loop(1, n_sp)
@@ -210,6 +275,26 @@
         )
         mixed_ref[:, u * LANES : (u + 1) * LANES] = mixed
 
+    for i in range(3, length):
+        relay(i)
+
+    for keep in keeps:
+        keep.wait()
+
+    @pl.loop(0, length)
+    def _(at):
+        for w in range(2):
+            source = weights[w][0]
+            to_side(w, at, source).wait()
+
+            @pl.when((at <= line) & (line + 1 < length))
+            def _():
+                to_line(w, at, line + 1, source, up_sem).wait_send()
+
+            @pl.when((at >= line) & (line >= 1))
+            def _():
+                to_line(w, at, line - 1, source, down_sem).wait_send()
+
     for u in range(len(units)):
 
         @pl.loop(1, n_sp)
@@ -219,15 +304,19 @@
                 copy(u, d, me + d).wait_send()
 
 
-def attention(n_sp, q, k, v, f, a, e, g, gain, own):
+def attention(n_sp, q, k, v, f, a, e, g, gain, own, first, second):
     T, channels = q.shape[1], q.shape[2]
     units = 2 * channels // LANES
     vmem = pl.BlockSpec(memory_space=pltpu.VMEM)
     return pl.pallas_call(
         functools.partial(attention_kernel, n_sp, (DS, DL)),
-        out_shape=jax.ShapeDtypeStruct((T, 2 * channels), jnp.bfloat16),
-        in_specs=[vmem] * 9,
-        out_specs=vmem,
+        out_shape=[
+            jax.ShapeDtypeStruct((T, 2 * channels), jnp.bfloat16),
+            jax.ShapeDtypeStruct((n_sp,) + first.shape, first.dtype),
+            jax.ShapeDtypeStruct((n_sp,) + second.shape, second.dtype),
+        ],
+        in_specs=[vmem] * 11,
+        out_specs=[vmem, pl.BlockSpec(memory_space=pl.ANY), pl.BlockSpec(memory_space=pl.ANY)],
         scratch_shapes=[
             pltpu.VMEM((units, T, LANES), jnp.float32),
             pltpu.VMEM((units, T, LANES), jnp.float32),
@@ -235,15 +324,17 @@
             pltpu.VMEM((n_sp, units, 2, LANES, LANES), jnp.bfloat16),
             pltpu.SemaphoreType.DMA((units, n_sp)),
             pltpu.SemaphoreType.DMA((units, n_sp)),
-        ],
+        ]
+        + [pltpu.SemaphoreType.DMA((2, n_sp // 2))] * 5
+        + [pltpu.SemaphoreType.DMA((2,))],
         compiler_params=pltpu.CompilerParams(
-            collective_id=0, has_side_effects=True, vmem_limit_bytes=40 * 2**20
+            collective_id=0, has_side_effects=True, vmem_limit_bytes=60 * 2**20
         ),
         cost_estimate=pl.CostEstimate(
-            flops=4 * 10**8, bytes_accessed=2**21, transcendentals=0
+            flops=15 * 10**10, bytes_accessed=2**28, transcendentals=0
         ),
         name="attention",
-    )(q, k, v, f, a, e, g, gain, own)
+    )(q, k, v, f, a, e, g, gain, own, first, second)
 
 
 def on_device(
@@ -263,11 +354,8 @@
     widening_matrix,
     shrinking_matrix,
 ):
-    gate_whole, up_whole = (
-        lax.all_gather(switching_matrix, "sp", axis=0, tiled=True),
-        lax.all_gather(widening_matrix, "sp", axis=0, tiled=True),
-    )
-    mixed = attention(
+    down_whole = lax.all_gather(shrinking_matrix, "sp", axis=1, tiled=True)
+    mixed, gate_whole, up_whole = attention(
         lax.axis_size("sp"),
         acceptance_query,
         cluster_lookup_matrix,
@@ -278,7 +366,11 @@
         result_switch_pair,
         attender_scaling_factor,
         present_item_factor,
-    )
+        switching_matrix,
+        widening_matrix,
+    )
+    gate_whole = gate_whole.reshape(-1, gate_whole.shape[2])
+    up_whole = up_whole.reshape(-1, up_whole.shape[2])
     partial_value = jnp.dot(
         mixed,
         final_mapping_matrix.reshape(-1, final_mapping_matrix.shape[2]),
@@ -305,7 +397,7 @@
     activated = (jax.nn.silu(gate_pre) * up_pre).astype(jnp.bfloat16)
     down_terms = jnp.dot(
         activated,
-        lax.all_gather(shrinking_matrix, "sp", axis=1, tiled=True),
+        down_whole,
         preferred_element_type=jnp.float32,
     )
     mixer = lax.psum_scatter(

time: 394 us -> 296 us (0.75)
  waiting for transfers between devices: 296 us -> 113 us
  Pallas kernels: 45.9 us -> 139 us
  local copies, waits for them, and re-layouts: 8.65 us -> 0.77 us
    all_gather x3 -> x1, waiting for transfers between devices: 240 us -> 55.5 us  [on_device(): down_whole = lax.all_gather(shrinking_matrix, 'sp', axis=1, tiled=True)]
    pallas_call x1, Pallas kernels: 45.9 us -> 139 us  [attention(): pl.pallas_call(functools.partial(attention_kernel, n_sp, (DS, DL)), out_s...]
    unnamed x20 -> x2, local copies, waits for them, and re-layouts: 7.89 us -> 0.01 us
  transfers between devices with their start and end apart: 5 -> 3, of which waited for: 5 -> 3; matrix products, arithmetic and copies ran while one was open for 1% -> 2% of each run, Pallas kernels for 0% -> 0%
where the time goes in v2:
time: 296 us
  Pallas kernels  139 us (47%)
  waiting for transfers between devices  113 us (38%)
  between operations  14.9 us (5%)
  blocking collectives  13.2 us (4%)
  matrix products  12.8 us (4%)
    pallas_call x1, Pallas kernels, attention(): pl.pallas_call(functools.partial(attention_kernel, n_sp, (DS, DL)), out_s...  139 us
    all_gather x1, waiting for transfers between devices, on_device(): down_whole = lax.all_gather(shrinking_matrix, 'sp', axis=1, tiled=True)  55.5 us
    reduce_scatter x1, waiting for transfers between devices, on_device(): lax.psum_scatter(partial_value.astype(jnp.bfloat16), 'tp', scatter_dimens...  36.6 us
    reduce_scatter x1, waiting for transfers between devices, on_device(): lax.psum_scatter(down_terms.astype(jnp.bfloat16), 'tp', scatter_dimension...  20 us
    all_gather x1, blocking collectives, on_device(): lax.all_gather(scaled.astype(jnp.bfloat16), 'tp', axis=1, tiled=True)  7.16 us
    dot_general x1, matrix products, on_device(): jnp.dot(activated, down_whole, preferred_element_type=jnp.float32)  7.06 us
    psum x1, blocking collectives, on_device(): square_total = lax.psum(jnp.sum(own_state * own_state, axis=1), 'tp')  6.06 us
  transfers between devices with their start and end apart: 3, of which 3 were waited for; matrix products, arithmetic and copies ran while one was open for 2% of the time, Pallas kernels for 0%

profile of v2, /device:TPU:0, one launch (start us, length us, event | category | flops | bytes accessed | tf_op | source)
XLA Modules:
  0.0 296.2 jit_solution(5747960441052812434)
XLA Ops:
  7.4 0.0 copy-start
  7.4 0.0 reduce-scatter.3.cloned.1.call-start
  7.4 139.0 %attention.1 = (bf16[128,512]{1,0:T(8,128)(2,1)}, bf16[8,256,1408]{2,1,0:T(8,128)(2,1)}, bf16[8,256,1408]{2,1,0:T(8,128)(2,1)}) custom-call(bf16[2,128,256]{2,1,0:T(8,128)(2,1)} %q_ref.1, bf16[2,128,256]{2,1,0:T(8,128)(2,1)} %k_ref.1, bf16[2,128,256]{2,1,0:T(8,128)(2,1)} %v_ref.1, bf16[2,128,256]{2,1,0:T(8,128)(2,1)} %f_ref.1, bf16[2,128,256]{2,1,0:T(8,128)(2,1)} %a_ref.1, ...), custom_call_target="tpu_custom_call" | custom-call | flops 149999992832 | bytes 268435456 | tf_op jit(solution)/shard_map/attention/pallas_call | solution.py:311
  146.3 0.0 copy-done
  146.3 2.2 convolution_convert_fusion
  148.5 0.0 reduce-scatter.3.cloned.1.call-update
  148.5 0.0 all-gather.2.cloned.1.call-start
  148.6 0.5 all-gather.2.cloned.1.call-update
  149.1 0.0 reduce-scatter.5.cloned.1.call-start
  149.2 0.8 dynamic_slice.7
  149.9 36.6 %reduce-scatter.3.cloned.1.call-done = bf16[128,512]{1,0:T(8,128)(2,1)} async-done(((bf16[128,2048]{1,0:T(8,128)(2,1)}), bf16[128,512]{1,0:T(8,128)(2,1)}) %reduce-scatter.3.cloned.1.call-update) | async-done | bytes 131088 | tf_op jit(solution)/shard_map/reduce_scatter | solution.py:382
  186.5 1.1 fusion.2
  187.6 6.1 %psum.7 = f32[128]{0:T(128)S(1)} all-reduce(f32[128]{0:T(128)S(1)} %get-tuple-element.11), channel_id=1, replica_groups=mesh['sp'=8,'tp'=4] {'tp'}, use_global_device_ids=true, to_apply=%region_2.0 | all-reduce | flops 128 | bytes 1024 | tf_op jit(solution)/shard_map/psum | solution.py:387
  193.7 0.1 fusion.4
  193.8 7.2 %all_gather.6 = bf16[128,2048]{1,0:T(8,128)(2,1)S(1)} all-gather(bf16[128,512]{1,0:T(8,128)(2,1)S(1)} %fusion.4), channel_id=1, replica_groups=mesh['sp'=8,'tp'=4] {'tp'}, dimensions={1}, use_global_device_ids=true | all-gather | bytes 655360 | tf_op jit(solution)/shard_map/all_gather | solution.py:394
  200.9 3.6 %fusion.7 = f32[128,1408]{1,0:T(8,128)S(1)} fusion(bf16[128,2048]{1,0:T(8,128)(2,1)S(1)} %all_gather.6, bf16[2048,1408]{1,0:T(8,128)(2,1)} %bitcast.11), kind=kOutput, calls=%fused_computation.15 | convolution fusion | flops 738197504 | bytes 7012352 | tf_op jit(solution)/shard_map/dot_general | solution.py:395
  204.6 55.5 %all-gather.2.cloned.1.call-done = bf16[1408,2048]{1,0:T(8,128)(2,1)} async-done(((bf16[1408,256]{1,0:T(8,128)(2,1)}), bf16[1408,2048]{1,0:T(8,128)(2,1)}) %all-gather.2.cloned.1.call-update) | async-done | bytes 5767184 | tf_op jit(solution)/shard_map/all_gather | solution.py:357
  260.1 7.1 %convolution_convert_fusion.1 = bf16[128,2048]{1,0:T(8,128)(2,1)} fusion(bf16[1408,2048]{1,0:T(8,128)(2,1)} %all-gather.2.cloned.1.call-done, bf16[128,2048]{1,0:T(8,128)(2,1)S(1)} %all_gather.6, bf16[2048,1408]{1,0:T(8,128)(2,1)} %bitcast.12, f32[128,1408]{1,0:T(8,128)S(1)} %fusion.7), kind=kOutput, calls=%fused_computation.3 | convolution fusion | flops 1477738496 | bytes 13303808 | tf_op jit(solution)/shard_map/dot_general | solution.py:398
  267.2 0.0 reduce-scatter.5.cloned.1.call-update
  267.2 20.0 %reduce-scatter.5.cloned.1.call-done = bf16[128,512]{1,0:T(8,128)(2,1)} async-done(((bf16[128,2048]{1,0:T(8,128)(2,1)}), bf16[128,512]{1,0:T(8,128)(2,1)}) %reduce-scatter.5.cloned.1.call-update) | async-done | bytes 131088 | tf_op jit(solution)/shard_map/reduce_scatter | solution.py:403
  287.2 1.6 fusion.5
  (1 shorter events, 0.0 us)
Async XLA Ops:
  7.4 139.0 %copy-start = (bf16[2,256,2048]{2,1,0:T(8,128)(2,1)S(1)}, bf16[2,256,2048]{2,1,0:T(8,128)(2,1)}, u32[]{:S(2)}) copy-start(bf16[2,256,2048]{2,1,0:T(8,128)(2,1)} %param.25) | copy-start | bytes 6291460
  7.4 179.1 %reduce-scatter.3.cloned.1.call-start = ((), (), s32[]{:S(2)}) async-start(), calls=%async_computation.2 | async-start | bytes 655360 | tf_op jit(solution)/shard_map/reduce_scatter | solution.py:382
  148.5 111.6 %all-gather.2.cloned.1.call-start = ((), (), s32[]{:S(2)}) async-start(), calls=%async_computation.3 | async-start | bytes 6488064 | tf_op jit(solution)/shard_map/all_gather | solution.py:357
  149.1 138.1 %reduce-scatter.5.cloned.1.call-start = ((), (), s32[]{:S(2)}) async-start(), calls=%async_computation.4 | async-start | bytes 655360 | tf_op jit(solution)/shard_map/reduce_scatter | solution.py:403
Sparse Core Ops, SparseCore 0:
  148.7 37.7 reduce-scatter.2
  267.3 19.8 reduce-scatter.4
Sparse Core Ops, SparseCore 1:
  151.1 109.0 all-gather.1
